TPU v7x, 32 devices: a whole 2x2x4 slice. The times are simulated.
32 devices in a mesh: kv: 16 (over z, y, x), tp: 2 (over core).
Axes of the slice: x: 2, y: 2, z: 4, core: 2. Of those that a mesh axis runs over, the one named last changes fastest.
Arguments:
- tokens: bfloat16 [64, 4096], P(None, 'kv'), may hold values from -12 to 12
- mix_gain: float32 [4096], P('kv'), may hold values from 0.1 to 1.9
- w_query: bfloat16 [4096, 2048], P('kv', 'tp'), may hold values from -0.09375 to 0.09375
- w_key: bfloat16 [4096, 2048], P('kv', 'tp'), may hold values from -0.09375 to 0.09375
- w_value: bfloat16 [4096, 2048], P('kv', 'tp'), may hold values from -0.09375 to 0.09375
- w_gate: bfloat16 [4096, 2048], P('kv', 'tp'), may hold values from -0.09375 to 0.09375
- w_beta: bfloat16 [4096, 16], P('kv', 'tp'), may hold values from -0.09375 to 0.09375
- w_decay: bfloat16 [4096, 16], P('kv', 'tp'), may hold values from -0.09375 to 0.09375
- decay_rate: float32 [16], P('tp'), may hold values from 0.05 to 3
- head_gain: float32 [128], replicated, may hold values from 0.1 to 1.9
- state: float32 [64, 16, 128, 128], P('kv', 'tp'), may hold values from -1.2 to 1.2
- w_out: bfloat16 [2048, 4096], P('tp', 'kv'), may hold values from -0.25 to 0.25
- mlp_gain: float32 [4096], P('kv'), may hold values from 0.1 to 1.9
- w_up: bfloat16 [4096, 16384], P('kv', 'tp'), may hold values from -0.09375 to 0.09375
- w_down: bfloat16 [16384, 4096], P('tp', 'kv'), may hold values from -0.046875 to 0.046875
Outputs:
- layer_out: bfloat16 [64, 4096], P(None, 'kv')
- new_state: float32 [64, 16, 128, 128], P('kv', 'tp')
All inputs are finite; a program needn't handle non-finite values.
Results may differ from a plain program's by a relative error of at most 0.017.
Values may be sent and summed in bfloat16 or wider, within the bound.
A program may use at most 64 MiB of HBM per device.

v0:
```python
import functools

import jax
import jax.numpy as jnp
from jax import lax
from jax.experimental import pallas as pl
from jax.experimental.pallas import tpu as pltpu
from jax.sharding import PartitionSpec as P


norm_eps = 1e-06


def rms_scale(values):
    return lax.rsqrt(jnp.mean(values * values, axis=-1, keepdims=True) + norm_eps)


def delta_update(
    query_pre, key_pre, value_pre, gate_pre, beta_pre, decay_pre, decay_rate, head_gain, state
):
    query = jax.nn.silu(query_pre)
    query = (
        query
        * lax.rsqrt(jnp.sum(query * query, axis=-1, keepdims=True) + norm_eps)
        * query.shape[-1] ** (-0.5)
    )
    keyed = jax.nn.silu(key_pre)
    keyed = keyed * lax.rsqrt(jnp.sum(keyed * keyed, axis=-1, keepdims=True) + norm_eps)
    valued = jax.nn.silu(value_pre)
    beta = jax.nn.sigmoid(beta_pre)
    decay = jnp.exp(-decay_rate * jax.nn.softplus(decay_pre))
    recalled = jnp.einsum("bhk,bhkv->bhv", keyed, state, precision=lax.Precision.HIGHEST)
    corrected = state - beta[:, :, None, None] * keyed[:, :, :, None] * recalled[:, :, None, :]
    new_state = (
        decay[:, :, None, None] * corrected
        + beta[:, :, None, None] * keyed[:, :, :, None] * valued[:, :, None, :]
    )
    read = jnp.einsum("bhkv,bhk->bhv", new_state, query, precision=lax.Precision.HIGHEST)
    mixed = read * rms_scale(read) * head_gain * jax.nn.silu(gate_pre)
    return (mixed, new_state)


def body(
    tokens,
    mix_gain,
    w_query,
    w_key,
    w_value,
    w_gate,
    w_beta,
    w_decay,
    decay_rate,
    head_gain,
    state,
    w_out,
    mlp_gain,
    w_up,
    w_down,
):
    f32 = jnp.float32
    bf16 = jnp.bfloat16
    local_rows = state.shape[0]
    heads_here = state.shape[1]
    head_size = state.shape[2]
    offset = lax.axis_index("kv") * local_rows
    D = tokens.shape[1] * lax.axis_size("kv")
    tok32 = tokens.astype(f32)
    squares = jnp.sum(tok32 * tok32, axis=1)
    gained = (tok32 * mix_gain).astype(bf16)
    joined = jnp.concatenate([w_query, w_key, w_value, w_gate], axis=1)
    rate_weights = jnp.concatenate([w_beta, w_decay], axis=1)
    main_term = jnp.dot(gained, joined, preferred_element_type=f32)
    rate_term = jnp.dot(gained, rate_weights, preferred_element_type=f32)
    energy_all = lax.psum(squares, "kv")
    main_part, rate_part = (
        lax.psum_scatter(main_term, "kv", scatter_dimension=0, tiled=True),
        lax.psum_scatter(rate_term, "kv", scatter_dimension=0, tiled=True),
    )
    energy = lax.dynamic_slice_in_dim(energy_all, offset, local_rows)
    scale = lax.rsqrt(energy / D + norm_eps)[:, None]
    main_part = (main_part * scale).reshape(local_rows, 4, heads_here, head_size)
    rate_part = rate_part * scale
    mixed, new_state = delta_update(
        main_part[:, 0],
        main_part[:, 1],
        main_part[:, 2],
        main_part[:, 3],
        rate_part[:, :heads_here],
        rate_part[:, heads_here:],
        decay_rate,
        head_gain,
        state,
    )
    mixed = mixed.reshape(local_rows, heads_here * head_size).astype(bf16)
    head_term = jnp.dot(
        lax.all_gather(mixed, "kv", axis=0, tiled=True), w_out, preferred_element_type=f32
    )
    attended = lax.psum(head_term.astype(jnp.bfloat16), "tp").astype(jnp.float32)
    residual = lax.optimization_barrier((tok32 + attended).astype(bf16)).astype(f32)
    squares_mid = jnp.sum(residual * residual, axis=1)
    gained_mid = (residual * mlp_gain).astype(bf16)
    up_term = jnp.dot(gained_mid, w_up, preferred_element_type=f32)
    up_part, energy_mid = lax.psum((up_term, squares_mid), "kv")
    scaled = up_part * lax.rsqrt(energy_mid / D + norm_eps)[:, None]
    down_term = jnp.dot(
        jnp.square(jax.nn.relu(scaled)).astype(bf16), w_down, preferred_element_type=f32
    )
    mixer = lax.psum(down_term.astype(jnp.bfloat16), "tp").astype(jnp.float32)
    layer_out = (residual + mixer).astype(bf16)
    return (layer_out, new_state)


MESH = pl.DeviceIdType.MESH
f32 = jnp.float32
bf16 = jnp.bfloat16


def inner_size(n):
    size = 1
    while size * size < n:
        size *= 2
    return size


def tiles(n, n_tp, inner, *args):
    tokens, state, w_up = args[0], args[10], args[13]
    rows, width = tokens.shape
    local, heads, size, _ = state.shape
    pairs = local * heads
    return (
        inner == 4
        and n_tp > 1
        and n % inner == 0
        and rows == n * local
        and width % 128 == 0
        and size == 128
        and heads == 8
        and pairs % 16 == 0
        and 128 % (2 * pairs) == 0
        and 128 % rows == 0
        and (rows // inner) % 16 == 0
        and w_up.shape[1] % (n * 128) == 0
        and n // inner > 1
    )


def remote(src, dst, send, recv, device):
    return pltpu.make_async_remote_copy(
        src_ref=src,
        dst_ref=dst,
        send_sem=send,
        recv_sem=recv,
        device_id=device,
        device_id_type=MESH,
    )


def kernel(
    n,
    n_tp,
    inner,
    tokens_h,
    mix_gain_h,
    w_query,
    w_key,
    w_value,
    w_gate,
    w_beta_h,
    w_decay_h,
    decay_rate_h,
    head_gain_h,
    state,
    w_out,
    mlp_gain_h,
    w_up,
    w_down,
    out,
    new_state_h,
    tokens,
    mix_gain,
    w_beta,
    w_decay,
    decay_rate,
    head_gain,
    mlp_gain,
    wp_v,
    state_v,
    new_state,
    w_out_v,
    w_up_v,
    w_down_v,
    a1,
    a1r,
    summed,
    a2,
    a2r,
    r1,
    r1r,
    rsum,
    r2,
    r2r,
    read_v,
    mix_v,
    mix_f,
    t1,
    u1,
    u1r,
    u2,
    u2r,
    en,
    hid,
    t2,
    small_sem,
    load_sem,
    state_sem,
    ns_sem,
    a1_s,
    a1_r,
    r1_s,
    r1_r,
    a2_s,
    a2_r,
    r2_s,
    r2_r,
    mx_s,
    mx_r,
    t1_s,
    t1_r,
    u1_s,
    u1_r,
    u2_s,
    u2_r,
    en_s,
    en_r,
    hz_s,
    hz_r,
    hp_s,
    hp_r,
    t2_s,
    t2_r,
):
    outer = n // inner
    rows, width = tokens.shape
    total_width = n * width
    local, heads, size, _ = state.shape
    pairs = local * heads
    group = rows // inner
    span = w_up.shape[1] // n
    me = lax.axis_index("kv")
    tp = lax.axis_index("tp")
    ours = lax.rem(me, inner)
    deep = me // inner
    sent = []

    def start(copy):
        copy.start()
        sent.append(copy)
        return copy

    def plane_peer(k):
        spot = lax.rem(ours + k, inner)
        return spot, {"kv": deep * inner + spot}

    def deep_peer(k):
        spot = lax.rem(deep + k, outer)
        return spot, {"kv": spot * inner + ours}

    small = []
    pairs_of = (
        (tokens_h, tokens),
        (mix_gain_h, mix_gain),
        (w_beta_h, w_beta),
        (w_decay_h, w_decay),
        (decay_rate_h, decay_rate),
        (head_gain_h, head_gain),
        (mlp_gain_h, mlp_gain),
    )
    for c, (src, dst) in enumerate(pairs_of):
        small.append(pltpu.make_async_copy(src, dst, small_sem.at[c]))
        small[-1].start()
    loads = []
    for c, ref in enumerate((w_query, w_key, w_value, w_gate)):
        loads.append(pltpu.make_async_copy(ref, wp_v.at[c], load_sem.at[c]))
    load_state = pltpu.make_async_copy(state, state_v, state_sem)
    load_out = pltpu.make_async_copy(w_out, w_out_v, load_sem.at[4])
    load_up = pltpu.make_async_copy(w_up, w_up_v, load_sem.at[5])
    load_down = pltpu.make_async_copy(w_down, w_down_v, load_sem.at[6])
    for copy in loads + [load_state, load_out, load_up, load_down]:
        copy.start()

    barrier = pltpu.get_barrier_semaphore()
    for k in range(1, outer):
        pl.semaphore_signal(
            barrier, inc=1, device_id=deep_peer(k)[1], device_id_type=MESH
        )
    for k in range(1, inner):
        pl.semaphore_signal(
            barrier, inc=1, device_id=plane_peer(k)[1], device_id_type=MESH
        )
    for k in range(1, n_tp):
        pl.semaphore_signal(
            barrier, inc=1, device_id={"tp": lax.rem(tp + k, n_tp)}, device_id_type=MESH
        )

    to_row = lax.broadcasted_iota(jnp.int32, (rows, rows), 0)
    from_row = lax.broadcasted_iota(jnp.int32, (rows, rows), 1)
    chosen = jnp.zeros((rows, rows), f32)
    for p in range(inner):
        for z in range(outer):
            begin = (p * outer + z) * local
            shift = begin - (z * inner + p) * local
            hit = (to_row - from_row == shift) & (to_row >= begin) & (to_row < begin + local)
            chosen = jnp.where(hit, 1.0, chosen)
    for copy in small:
        copy.wait()
    tok32 = tokens[...].astype(f32)
    moved = jnp.dot(chosen.astype(bf16), tokens[...], preferred_element_type=f32)
    gained = (moved * mix_gain[...]).astype(bf16)
    lane = lax.broadcasted_iota(jnp.int32, (heads, 128), 1)
    sub = lax.broadcasted_iota(jnp.int32, (heads, 128), 0)
    rate_weights = jnp.concatenate(
        [
            w_beta[...].astype(f32),
            w_decay[...].astype(f32),
            jnp.zeros((128 - 2 * heads, width), f32),
        ],
        axis=0,
    ).astype(bf16)
    rate = lax.dot_general(
        gained, rate_weights, (((1,), (1,)), ((), ())), preferred_element_type=f32
    )
    energy_col = jnp.sum(moved * moved, axis=1, keepdims=True)
    lanes = lax.broadcasted_iota(jnp.int32, (rows, 128), 1)
    rate = rate + jnp.where(lanes == 2 * heads, energy_col, 0.0)
    for p in range(inner):
        r1[p] = rate[p * group : (p + 1) * group]

    pl.semaphore_wait(barrier, outer - 1 + inner - 1 + n_tp - 1)

    first = {}
    for c in range(4):
        loads[c].wait()
        term = jnp.dot(gained, wp_v[c], preferred_element_type=f32).astype(bf16)
        for p in range(inner):
            a1[c, p] = term[p * group : (p + 1) * group]
        for k in range(1, inner):
            spot, device = plane_peer(k)
            first[c, k] = start(
                remote(a1.at[c, spot], a1r.at[c, k], a1_s.at[c, k], a1_r.at[c, k], device)
            )
        if c == 0:
            for k in range(1, inner):
                spot, device = plane_peer(k)
                first["r", k] = start(
                    remote(r1.at[spot], r1r.at[k], r1_s.at[k], r1_r.at[k], device)
                )

    second = {}
    for c in range(4):
        total = a1[c, ours].astype(f32)
        for k in range(1, inner):
            first[c, k].wait_recv()
            total = total + a1r[c, k].astype(f32)
        base = c * group * heads
        for h in range(heads):
            summed[pl.ds(base + h, group, stride=heads), :] = total[
                :, h * size : (h + 1) * size
            ]
        for z in range(outer):
            a2[c, z] = summed[pl.ds(base + z * pairs, pairs), :].astype(bf16)
        for k in range(1, outer):
            spot, device = deep_peer(k)
            second[c, k] = start(
                remote(a2.at[c, spot], a2r.at[c, k], a2_s.at[c, k], a2_r.at[c, k], device)
            )
        if c == 0:
            total = r1[ours]
            for k in range(1, inner):
                first["r", k].wait_recv()
                total = total + r1r[k]
            rsum[...] = total
            r2[...] = jnp.zeros(r2.shape, f32)
            for z in range(outer):
                r2[z, 0:local, :] = rsum[z * local : (z + 1) * local, :]
            for k in range(1, outer):
                spot, device = deep_peer(k)
                second["r", k] = start(
                    remote(r2.at[spot], r2r.at[k], r2_s.at[k], r2_r.at[k], device)
                )

    rate = r2[deep]
    for k in range(1, outer):
        second["r", k].wait_recv()
        rate = rate + r2r[k]

    def column(r, first_lane, step):
        row = jnp.broadcast_to(rate[r : r + 1, :], (heads, 128))
        return jnp.sum(
            jnp.where(lane == first_lane + step * sub, row, 0.0), axis=1, keepdims=True
        )

    def columns(first_lane, step):
        return jnp.concatenate([column(r, first_lane, step) for r in range(local)], axis=0)

    scale = lax.rsqrt(columns(2 * heads, 0) / total_width + norm_eps)
    beta = jax.nn.sigmoid(columns(0, 1) * scale)
    decay_pre = columns(heads, 1) * scale
    rate_row = jnp.broadcast_to(decay_rate[...], (heads, heads))
    diagonal = lax.broadcasted_iota(jnp.int32, (heads, heads), 0) == lax.broadcasted_iota(
        jnp.int32, (heads, heads), 1
    )
    rate_one = jnp.sum(jnp.where(diagonal, rate_row, 0.0), axis=1, keepdims=True)
    rates = jnp.concatenate([rate_one] * local, axis=0)
    softplus = jnp.maximum(decay_pre, 0.0) + jnp.log1p(jnp.exp(-jnp.abs(decay_pre)))
    decay = jnp.exp(-rates * softplus)
    beta_b = jnp.broadcast_to(beta, (pairs, size))
    decay_b = jnp.broadcast_to(decay, (pairs, size))

    pre = []
    for c in range(4):
        begin = pl.multiple_of(c * group * heads + deep * pairs, pairs)
        total = summed[pl.ds(begin, pairs), :]
        for k in range(1, outer):
            second[c, k].wait_recv()
            total = total + a2r[c, k].astype(f32)
        pre.append(total * scale)
    query = jax.nn.silu(pre[0])
    query = (
        query
        * lax.rsqrt(jnp.sum(query * query, axis=-1, keepdims=True) + norm_eps)
        * size ** (-0.5)
    )
    keyed = jax.nn.silu(pre[1])
    keyed = keyed * lax.rsqrt(jnp.sum(keyed * keyed, axis=-1, keepdims=True) + norm_eps)
    valued = jax.nn.silu(pre[2])
    turned = jnp.concatenate([keyed, query] * (128 // (2 * pairs)), axis=0).T
    load_state.wait()
    stores = []
    for r in range(local):
        for h in range(heads):
            i = r * heads + h
            key_col = turned[:, i : i + 1]
            query_col = turned[:, pairs + i : pairs + i + 1]
            old = state_v[r, h]
            decay_row = decay_b[i : i + 1]
            recalled = jnp.sum(key_col * old, axis=0, keepdims=True)
            write = beta_b[i : i + 1] * (valued[i : i + 1] - decay_row * recalled)
            new = decay_row * old + key_col * write
            new_state[r, h] = new
            read_v[i : i + 1, :] = jnp.sum(query_col * new, axis=0, keepdims=True)
        stores.append(
            pltpu.make_async_copy(new_state.at[r], new_state_h.at[r], ns_sem.at[r])
        )
        stores[-1].start()
    read = read_v[...]
    mixed = read * rms_scale(read) * head_gain[...] * jax.nn.silu(pre[3])
    mix_v[me] = mixed.astype(bf16)
    for k in range(1, n):
        start(
            remote(
                mix_v.at[me],
                mix_v.at[me],
                mx_s.at[k],
                mx_r.at[k],
                {"kv": lax.rem(me + k, n)},
            )
        )
    load_out.wait()
    for k in range(1, n):
        came = lax.rem(me + n - k, n)
        remote(
            mix_v.at[came], mix_v.at[came], mx_s.at[k], mx_r.at[k], {"kv": lax.rem(me + k, n)}
        ).wait_recv()
    for d in range(n):
        mix_f[d * pairs : (d + 1) * pairs, :] = mix_v[d].astype(f32)
    joined = jnp.concatenate(
        [mix_f[pl.ds(h, rows, stride=heads), :].astype(bf16) for h in range(heads)], axis=1
    )

    def over_tp(term, slots, send, recv):
        slots[tp] = term.astype(bf16)
        for k in range(1, n_tp):
            start(
                remote(
                    slots.at[tp],
                    slots.at[tp],
                    send.at[k],
                    recv.at[k],
                    {"tp": lax.rem(tp + k, n_tp)},
                )
            )
        for k in range(1, n_tp):
            came = lax.rem(tp + n_tp - k, n_tp)
            remote(
                slots.at[came],
                slots.at[came],
                send.at[k],
                recv.at[k],
                {"tp": lax.rem(tp + k, n_tp)},
            ).wait_recv()
        total = slots[0].astype(f32)
        for t in range(1, n_tp):
            total = total + slots[t].astype(f32)
        return total

    attended = over_tp(
        jnp.dot(joined, w_out_v[...], preferred_element_type=f32), t1, t1_s, t1_r
    )
    residual = (tok32 + attended).astype(bf16).astype(f32)
    gained_mid = (residual * mlp_gain[...]).astype(bf16)

    load_up.wait()
    ups = {}
    order = list(range(1, outer)) + [0]
    for step, j in enumerate(order):
        z = lax.rem(deep + j, outer)
        for k in list(range(1, inner)) + [0]:
            spot, device = plane_peer(k)
            begin = pl.multiple_of((spot * outer + z) * span, 128)
            term = jnp.dot(
                gained_mid, w_up_v[:, pl.ds(begin, span)], preferred_element_type=f32
            )
            u1[j, k] = term.astype(bf16)
            if k:
                ups[j, k] = start(
                    remote(u1.at[j, k], u1r.at[j, k], u1_s.at[j, k], u1_r.at[j, k], device)
                )
        if step == 0:
            squares = jnp.concatenate([residual * residual] * (128 // rows), axis=0)
            en[me] = lax.dot_general(
                jnp.ones((8, width), f32),
                squares,
                (((1,), (1,)), ((), ())),
                precision=lax.Precision.HIGHEST,
                preferred_element_type=f32,
            )
            for k in range(1, n):
                start(
                    remote(
                        en.at[me],
                        en.at[me],
                        en_s.at[k],
                        en_r.at[k],
                        {"kv": lax.rem(me + k, n)},
                    )
                )

    def plane_sum(j):
        total = u1[j, 0].astype(f32)
        for k in range(1, inner):
            ups[j, k].wait_recv()
            total = total + u1r[j, k].astype(f32)
        return total

    across = {}
    for j in range(1, outer):
        u2[j] = plane_sum(j).astype(bf16)
        _, device = deep_peer(j)
        across[j] = start(remote(u2.at[j], u2r.at[j], u2_s.at[j], u2_r.at[j], device))
    up = plane_sum(0)
    for k in range(1, n):
        came = lax.rem(me + n - k, n)
        remote(
            en.at[came], en.at[came], en_s.at[k], en_r.at[k], {"kv": lax.rem(me + k, n)}
        ).wait_recv()
    energy = en[0]
    for d in range(1, n):
        energy = energy + en[d]
    spread = jnp.broadcast_to(energy[0:1, :], (rows, 128))
    at_row = lax.broadcasted_iota(jnp.int32, (rows, 128), 0)
    energy_mid = jnp.sum(jnp.where(lanes == at_row, spread, 0.0), axis=1, keepdims=True)
    scale_mid = lax.rsqrt(energy_mid / total_width + norm_eps)
    for j in range(1, outer):
        across[j].wait_recv()
        up = up + u2r[j].astype(f32)
    mine = ours * outer + deep
    hid[mine] = jnp.square(jax.nn.relu(up * scale_mid)).astype(bf16)

    half = rows // 2
    flat = lax.rem(ours, 2)
    next_spot = (ours + 1 - 2 * flat, lax.rem(ours + 2, inner))
    corner = lax.rem(next_spot[0] + 2, inner)
    nearby = [{"kv": deep * inner + spot} for spot in next_spot]

    def block_of(spot, j):
        return spot * outer + lax.rem(deep + outer - j, outer)

    def near_copy(spot, j, side):
        block = hid.at[block_of(spot, j)]
        return remote(block, block, hp_s.at[j, side], hp_r.at[j, side], nearby[side])

    def corner_copy(spot, j, side):
        block = hid.at[block_of(spot, j), pl.ds((1 - side) * half, half)]
        return remote(block, block, hp_s.at[j, 2 + side], hp_r.at[j, 2 + side], nearby[side])

    def down(block):
        begin = pl.multiple_of(block * span, 128)
        return jnp.dot(
            hid[block], w_down_v[pl.ds(begin, span), :], preferred_element_type=f32
        )

    def pass_on(j):
        for side in range(2):
            near_copy(next_spot[side], j, side).wait_recv()
            start(corner_copy(next_spot[side], j, 1 - side))

    for side in range(2):
        start(near_copy(ours, 0, side))
    for k in range(1, outer):
        _, device = deep_peer(k)
        start(remote(hid.at[mine], hid.at[mine], hz_s.at[k], hz_r.at[k], device))
    load_down.wait()
    total = down(mine)
    for j in range(1, outer):
        block = block_of(ours, j)
        _, device = deep_peer(j)
        remote(hid.at[block], hid.at[block], hz_s.at[j], hz_r.at[j], device).wait_recv()
        for side in range(2):
            start(near_copy(ours, j, side))
        pass_on(j - 1)
        total = total + down(block)
    pass_on(outer - 1)
    for j in range(outer):
        for side in range(2):
            total = total + down(block_of(next_spot[side], j))
    for j in range(outer):
        for side in range(2):
            corner_copy(corner, j, side).wait_recv()
        total = total + down(block_of(corner, j))
    mixer = over_tp(total, t2, t2_s, t2_r)
    out[...] = (residual + mixer).astype(bf16)
    for copy in sent:
        copy.wait_send()
    for copy in stores:
        copy.wait()


def fused(n, n_tp, inner, *args):
    (
        tokens,
        mix_gain,
        w_query,
        w_key,
        w_value,
        w_gate,
        w_beta,
        w_decay,
        decay_rate,
        head_gain,
        state,
        w_out,
        mlp_gain,
        w_up,
        w_down,
    ) = args
    outer = n // inner
    rows, width = tokens.shape
    local, heads, size, _ = state.shape
    pairs = local * heads
    group = rows // inner
    span = w_up.shape[1] // n
    wide = heads * size
    pad = -(-local // 8) * 8
    hbm = pl.BlockSpec(memory_space=pltpu.HBM)
    vmem = pl.BlockSpec(memory_space=pltpu.VMEM)
    V = pltpu.VMEM
    S = pltpu.SemaphoreType.DMA
    pair = lambda *shape: [S(shape), S(shape)]
    scratch = [
        V((rows, width), bf16),
        V((1, width), f32),
        V((heads, width), bf16),
        V((heads, width), bf16),
        V((1, heads), f32),
        V((1, size), f32),
        V((1, width), f32),
        V((4, width, wide), bf16),
        V(state.shape, f32),
        V(state.shape, f32),
        V(w_out.shape, bf16),
        V(w_up.shape, bf16),
        V(w_down.shape, bf16),
        V((4, inner, group, wide), bf16),
        V((4, inner, group, wide), bf16),
        V((4 * group * heads, size), f32),
        V((4, outer, pairs, size), bf16),
        V((4, outer, pairs, size), bf16),
        V((inner, group, 128), f32),
        V((inner, group, 128), f32),
        V((group, 128), f32),
        V((outer, pad, 128), f32),
        V((outer, pad, 128), f32),
        V((pairs, size), f32),
        V((n, pairs, size), bf16),
        V((n * pairs, size), f32),
        V((n_tp, rows, width), bf16),
        V((outer, inner, rows, span), bf16),
        V((outer, inner, rows, span), bf16),
        V((outer, rows, span), bf16),
        V((outer, rows, span), bf16),
        V((n, 8, 128), f32),
        V((n, rows, span), bf16),
        V((n_tp, rows, width), bf16),
        S((7,)),
        S((7,)),
        S,
        S((local,)),
    ]
    for shape in (
        (4, inner),
        (inner,),
        (4, outer),
        (outer,),
        (n,),
        (n_tp,),
        (outer, inner),
        (outer,),
        (n,),
        (outer,),
        (outer, inner),
        (n_tp,),
    ):
        scratch += pair(*shape)
    return pl.pallas_call(
        functools.partial(kernel, n, n_tp, inner),
        out_shape=(
            jax.ShapeDtypeStruct((rows, width), bf16),
            jax.ShapeDtypeStruct(state.shape, f32),
        ),
        in_specs=[hbm] * 15,
        out_specs=(vmem, hbm),
        scratch_shapes=scratch,
        compiler_params=pltpu.CompilerParams(
            collective_id=0, has_side_effects=True, vmem_limit_bytes=60 * 1024 * 1024
        ),
    )(
        tokens,
        mix_gain.reshape(1, width),
        w_query,
        w_key,
        w_value,
        w_gate,
        w_beta.T,
        w_decay.T,
        decay_rate.reshape(1, heads),
        head_gain.reshape(1, size),
        state,
        w_out,
        mlp_gain.reshape(1, width),
        w_up,
        w_down,
    )


def solution(mesh):
    n, n_tp = mesh.shape["kv"], mesh.shape["tp"]
    inner = inner_size(n)

    def step(*args):
        if tiles(n, n_tp, inner, *args):
            return fused(n, n_tp, inner, *args)
        return body(*args)

    return jax.shard_map(
        step,
        mesh=mesh,
        in_specs=(
            P(None, "kv"),
            P("kv"),
            P("kv", "tp"),
            P("kv", "tp"),
            P("kv", "tp"),
            P("kv", "tp"),
            P("kv", "tp"),
            P("kv", "tp"),
            P("tp"),
            P(),
            P("kv", "tp", None, None),
            P("tp", "kv"),
            P("kv"),
            P("kv", "tp"),
            P("tp", "kv"),
        ),
        out_specs=(P(None, "kv"), P("kv", "tp", None, None)),
        check_vma=False,
    )
```

profile of v0, /device:TPU:1, one launch (start us, length us, event | category | flops | bytes accessed | tf_op | source)
XLA Modules:
  0.0 65.8 jit_solution(13671450286575662007)
XLA Ops:
  0.6 60.7 %shard_map.158 = (bf16[64,256]{1,0:T(8,128)(2,1)}, f32[4,8,128,128]{3,2,1,0:T(8,128)}) custom-call(bf16[64,256]{1,0:T(8,128)(2,1)} %tokens_h.1, f32[1,256]{1,0:T(1,128)} %bitcast.8, bf16[256,1024]{1,0:T(8,128)(2,1)} %w_query.1, bf16[256,1024]{1,0:T(8,128)(2,1)} %w_key.1, bf16[256,1024]{1,0:T(8,128)(2,1)} %w_value.1, bf16[256,1024]{1,0:T(8,128)(2,1)} %w_gate.1, ...), custom_call_target="tpu_custom_call" | custom-call | tf_op jit(solution)/shard_map/pallas_call | solution.py:724
  61.3 1.4 %copy.19 = bf16[64,256]{1,0:T(8,128)(2,1)} copy(bf16[64,256]{1,0:T(8,128)(2,1)} %get-tuple-element.4) | data formatting | bytes 65536
  62.7 3.1 %copy.20 = f32[4,8,128,128]{3,2,1,0:T(8,128)} copy(f32[4,8,128,128]{3,2,1,0:T(8,128)} %get-tuple-element.5) | data formatting | bytes 4194304
where the time goes:
time: 66 us; the launch traced here: 65.8 us
  Pallas kernels  60.7 us (92%)
  local copies, waits for them, and re-layouts  4.51 us (7%)
    pallas_call x1, Pallas kernels, fused(): pl.pallas_call(functools.partial(kernel, n, n_tp, inner), out_shape=(jax....  60.7 us
    unnamed x2, local copies, waits for them, and re-layouts  4.51 us

commit v1 on v0

--- a/solution.py
+++ b/solution.py
@@ -175,7 +175,7 @@
     w_up,
     w_down,
     out,
-    new_state_h,
+    new_state,
     tokens,
     mix_gain,
     w_beta,
@@ -185,7 +185,6 @@
     mlp_gain,
     wp_v,
     state_v,
-    new_state,
     w_out_v,
     w_up_v,
     w_down_v,
@@ -213,7 +212,6 @@
     small_sem,
     load_sem,
     state_sem,
-    ns_sem,
     a1_s,
     a1_r,
     r1_s,
@@ -285,7 +283,7 @@
     load_out = pltpu.make_async_copy(w_out, w_out_v, load_sem.at[4])
     load_up = pltpu.make_async_copy(w_up, w_up_v, load_sem.at[5])
     load_down = pltpu.make_async_copy(w_down, w_down_v, load_sem.at[6])
-    for copy in loads + [load_state, load_out, load_up, load_down]:
+    for copy in loads:
         copy.start()
 
     barrier = pltpu.get_barrier_semaphore()
@@ -313,6 +311,8 @@
             chosen = jnp.where(hit, 1.0, chosen)
     for copy in small:
         copy.wait()
+    for copy in [load_state, load_out, load_up, load_down]:
+        copy.start()
     tok32 = tokens[...].astype(f32)
     moved = jnp.dot(chosen.astype(bf16), tokens[...], preferred_element_type=f32)
     gained = (moved * mix_gain[...]).astype(bf16)
@@ -435,7 +435,6 @@
     valued = jax.nn.silu(pre[2])
     turned = jnp.concatenate([keyed, query] * (128 // (2 * pairs)), axis=0).T
     load_state.wait()
-    stores = []
     for r in range(local):
         for h in range(heads):
             i = r * heads + h
@@ -448,10 +447,6 @@
             new = decay_row * old + key_col * write
             new_state[r, h] = new
             read_v[i : i + 1, :] = jnp.sum(query_col * new, axis=0, keepdims=True)
-        stores.append(
-            pltpu.make_async_copy(new_state.at[r], new_state_h.at[r], ns_sem.at[r])
-        )
-        stores[-1].start()
     read = read_v[...]
     mixed = read * rms_scale(read) * head_gain[...] * jax.nn.silu(pre[3])
     mix_v[me] = mixed.astype(bf16)
@@ -631,7 +626,15 @@
     out[...] = (residual + mixer).astype(bf16)
     for copy in sent:
         copy.wait_send()
-    for copy in stores:
+
+
+def write_back(out_v, state_v, out, state, sem):
+    copies = [pltpu.make_async_copy(out_v, out, sem.at[0])]
+    for r in range(state_v.shape[0]):
+        copies.append(pltpu.make_async_copy(state_v.at[r], state.at[r], sem.at[1 + r]))
+    for copy in copies:
+        copy.start()
+    for copy in copies:
         copy.wait()
 
 
@@ -676,7 +679,6 @@
         V((1, width), f32),
         V((4, width, wide), bf16),
         V(state.shape, f32),
-        V(state.shape, f32),
         V(w_out.shape, bf16),
         V(w_up.shape, bf16),
         V(w_down.shape, bf16),
@@ -704,7 +706,6 @@
         S((7,)),
         S((7,)),
         S,
-        S((local,)),
     ]
     for shape in (
         (4, inner),
@@ -721,14 +722,11 @@
         (n_tp,),
     ):
         scratch += pair(*shape)
-    return pl.pallas_call(
+    held = pl.pallas_call(
         functools.partial(kernel, n, n_tp, inner),
-        out_shape=(
-            jax.ShapeDtypeStruct((rows, width), bf16),
-            jax.ShapeDtypeStruct(state.shape, f32),
-        ),
+        out_shape=(pltpu.VMEM((rows, width), bf16), pltpu.VMEM(state.shape, f32)),
         in_specs=[hbm] * 15,
-        out_specs=(vmem, hbm),
+        out_specs=(vmem, vmem),
         scratch_shapes=scratch,
         compiler_params=pltpu.CompilerParams(
             collective_id=0, has_side_effects=True, vmem_limit_bytes=60 * 1024 * 1024
@@ -750,6 +748,16 @@
         w_up,
         w_down,
     )
+    return pl.pallas_call(
+        write_back,
+        out_shape=(
+            jax.ShapeDtypeStruct((rows, width), bf16),
+            jax.ShapeDtypeStruct(state.shape, f32),
+        ),
+        in_specs=[vmem, vmem],
+        out_specs=(hbm, hbm),
+        scratch_shapes=[S((1 + local,))],
+    )(*[pltpu.with_memory_space_constraint(x, pltpu.VMEM) for x in held])
 
 
 def solution(mesh):

time: 66 us -> 61.3 us (0.929)
  local copies, waits for them, and re-layouts: 4.51 us -> 0 us
    unnamed x2 -> x0, local copies, waits for them, and re-layouts: 4.51 us -> none
    pallas_call x1 -> x2, Pallas kernels: 60.7 us -> 60.5 us  [the longest x1 59.1 us: fused(): pl.pallas_call(functools.partial(kernel, n, n_tp, inner), out_shape=(pltp...]
where the time goes in v1:
time: 61.3 us; the launch traced here: 61.1 us
  Pallas kernels  60.5 us (99%)
  between operations  0.64 us (1%)
    pallas_call x1, Pallas kernels, fused(): pl.pallas_call(functools.partial(kernel, n, n_tp, inner), out_shape=(pltp...  59.1 us
    pallas_call x1, Pallas kernels, fused(): pl.pallas_call(write_back, out_shape=(jax.ShapeDtypeStruct((rows, width),...  1.37 us

profile of v1, /device:TPU:1, one launch (start us, length us, event | category | flops | bytes accessed | tf_op | source)
XLA Modules:
  0.0 61.1 jit_solution(16013968952090855464)
XLA Ops:
  0.6 59.1 %shard_map.158 = (bf16[64,256]{1,0:T(8,128)(2,1)S(1)}, f32[4,8,128,128]{3,2,1,0:T(8,128)S(1)}) custom-call(bf16[64,256]{1,0:T(8,128)(2,1)} %tokens_h.1, f32[1,256]{1,0:T(1,128)} %bitcast.8, bf16[256,1024]{1,0:T(8,128)(2,1)} %w_query.1, bf16[256,1024]{1,0:T(8,128)(2,1)} %w_key.1, bf16[256,1024]{1,0:T(8,128)(2,1)} %w_value.1, bf16[256,1024]{1,0:T(8,128)(2,1)} %w_gate.1, ...), custom_call_target="tpu_custom_call" | custom-call | tf_op jit(solution)/shard_map/pallas_call | solution.py:725
  59.7 1.4 %shard_map.159 = (bf16[64,256]{1,0:T(8,128)(2,1)}, f32[4,8,128,128]{3,2,1,0:T(8,128)}) custom-call(bf16[64,256]{1,0:T(8,128)(2,1)S(1)} %get-tuple-element.4.out_v, f32[4,8,128,128]{3,2,1,0:T(8,128)S(1)} %get-tuple-element.5.state_v), custom_call_target="tpu_custom_call" | custom-call | tf_op jit(solution)/shard_map/pallas_call | solution.py:751
